TPU v7x, 32 devices: a whole 2x2x4 slice. The times are simulated.
32 devices in a mesh: grp: 2 (over y), sp: 4 (over z), tp: 4 (over x, core).
Axes of the slice: x: 2, y: 2, z: 4, core: 2. Of those that a mesh axis runs over, the one named last changes fastest.
Arguments:
- gate_in: bfloat16 [4096, 1536], P(('grp', 'sp'), 'tp'), parts along dimension 0, may hold values from -6 to 6
- mult_in: bfloat16 [4096, 1536], P(('grp', 'sp'), 'tp'), parts along dimension 0, may hold values from -6 to 6
- value_in: bfloat16 [4096, 1536], P(('grp', 'sp'), 'tp'), parts along dimension 0, may hold values from -6 to 6
- doc_ids: int32 [4096], P(('grp', 'sp')), parts along dimension 0, may hold values from 0 to 1, never falling along the last dimension, each value on 1 to 1536 neighbouring positions
- conv_taps: bfloat16 [3, 1536], P(None, 'tp'), may hold values from -3 to 3
- out_proj: bfloat16 [1536, 2048], P('tp'), may hold values from -0.15625 to 0.15625
- resid: bfloat16 [4096, 2048], P(('grp', 'sp', 'tp')), parts along dimension 0, may hold values from -6 to 6
- norm1_gain: float32 [2048], replicated, may hold values from 0.1 to 1.9
- norm1_bias: float32 [2048], replicated, may hold values from -1.5 to 1.5
- expert_ids: int32 [4096, 2], P(('grp', 'sp', 'tp')), parts along dimension 0, may hold values from 0 to 3, all different within a row; in each aligned block of 128 rows (0 to 127, 128 to 255, ...) at most 80 rows name the same one
- expert_wts: float32 [4096, 2], P(('grp', 'sp', 'tp')), parts along dimension 0, may hold values from 0.1 to 1
- w_gate: bfloat16 [4, 2048, 3072], P('sp', None, 'tp'), may hold values from -0.125 to 0.125
- w_up: bfloat16 [4, 2048, 3072], P('sp', None, 'tp'), may hold values from -0.125 to 0.125
- w_down: bfloat16 [4, 3072, 2048], P('sp', 'tp'), may hold values from -0.21582031 to 0.21582031
- norm2_gain: float32 [2048], replicated, may hold values from 0.1 to 1.9
- norm2_bias: float32 [2048], replicated, may hold values from -1.5 to 1.5
Outputs:
- result: bfloat16 [4096, 2048], P(('grp', 'sp', 'tp')), parts along dimension 0
There are 2 independent parts, one for each index of `grp`. A program takes and returns all parts, laid end to end along the dimension named above; an argument that names none is the same for every part. Nothing has to cross between parts.
Inputs may be any that keep to these rules, and one draw needn't show every extreme that they name: `doc_ids`: never falling along the sequence; each document has 1 to 1536 positions and one has exactly 1536. `expert_ids`: each row names 2 different experts. Among the rows of one device no expert is named more than 80 times, and in some device's rows some expert is named exactly 80 times.
All inputs are finite; a program needn't handle non-finite values.
Results may differ from a plain program's by a relative error of at most 0.0095.
Values may be sent and summed in bfloat16 or wider, within the bound.
A program may use at most 128 MiB of HBM per device.

v0:
```python
import functools

import jax
import jax.numpy as jnp
from jax import lax
from jax.experimental import pallas as pl
from jax.experimental.pallas import tpu as pltpu
from jax.sharding import PartitionSpec as P

residual_scale = 2.0**0.5
norm_eps = 1e-05
MESH = pl.DeviceIdType.MESH
f32, bf16 = jnp.float32, jnp.bfloat16


def layer_norm(pre, gain, bias):
    center = pre - jnp.mean(pre, axis=-1, keepdims=True)
    spread = jnp.mean(center * center, axis=-1, keepdims=True)
    return center * lax.rsqrt(spread + norm_eps) * gain + bias


def remote(src, dst, send, recv, **where):
    return pltpu.make_async_remote_copy(
        src_ref=src, dst_ref=dst, send_sem=send, recv_sem=recv, device_id=where, device_id_type=MESH
    )


def kernel(
    experts, slots, piece,
    gate_h, mult_h, value_h, docs_h, taps, proj_h, resid_h, gain1, bias1, ids, wts,
    w_gate_h, w_up_h, w_down_h, gain2, bias2,
    out,
    gate, mult, value, docs, proj, resid, w_gate, w_up, w_down,
    edge_m, edge_v, edge_d, ext, ext_docs, heads,
    send1, got1, send2, got2, own, hidden, slot_of, weight_of,
    packed, rows, part, hid, sum_in, sum_send, cross_in, done_out, back, picks,
    local, edge_s, edge_r, mix_s, mix_r,
    zs, zr, xs, xr, bs, br, cs, cr, r1s, r1r, r2s, r2r, r3s, r3r,
):
    s, t = lax.axis_index("sp"), lax.axis_index("tp")
    hi, lo = t // 2, t % 2
    sib, far = hi * 2 + (1 - lo), (1 - hi) * 2 + lo
    count, model = resid.shape
    length, channels = mult.shape
    taps_n = taps.shape[0]
    top = ids.shape[0]

    loads = [
        pltpu.make_async_copy(a, b, local.at[i])
        for i, (a, b) in enumerate(
            [(mult_h, mult), (value_h, value), (docs_h, docs), (gate_h, gate), (proj_h, proj),
             (resid_h, resid), (w_gate_h, w_gate), (w_up_h, w_up), (w_down_h, w_down)]
        )
    ]
    for c in loads:
        c.start()

    barrier = pltpu.get_barrier_semaphore()

    def greet(d, _):
        pl.semaphore_signal(barrier, inc=1, device_id={"sp": (s + d) % experts}, device_id_type=MESH)
        return 0

    lax.fori_loop(1, experts, greet, 0)
    pl.semaphore_signal(barrier, inc=1, device_id={"tp": sib}, device_id_type=MESH)
    pl.semaphore_signal(barrier, inc=1, device_id={"tp": far}, device_id_type=MESH)
    pl.semaphore_wait(barrier, experts + 1)

    nxt = (s + 1) % experts
    edges = [
        remote(mult_h.at[pl.ds(length - 16, 16)], edge_m, edge_s.at[0], edge_r.at[0], sp=nxt),
        remote(value_h.at[pl.ds(length - 16, 16)], edge_v, edge_s.at[1], edge_r.at[1], sp=nxt),
        remote(docs_h.at[pl.ds(length - 8, 8)], edge_d, edge_s.at[2], edge_r.at[2], sp=nxt),
    ]
    for c in edges:
        c.start()

    padded = slot_of.shape[0]
    expert_no = lax.broadcasted_iota(jnp.int32, (padded, count), 0)
    chosen = jnp.zeros((padded, count), f32)
    weight = jnp.zeros((padded, count), f32)
    for k in range(top):
        same = ids[k : k + 1, :] == expert_no
        chosen = chosen + jnp.where(same, 1.0, 0.0)
        weight = weight + jnp.where(same, wts[k : k + 1, :], 0.0)
    before = lax.broadcasted_iota(jnp.int32, (count, count), 0) < lax.broadcasted_iota(
        jnp.int32, (count, count), 1
    )
    rank = jnp.dot(chosen.astype(bf16), jnp.where(before, 1.0, 0.0).astype(bf16), preferred_element_type=f32)
    slot_of[...] = jnp.where(chosen > 0.5, rank, -1.0)
    weight_of[...] = weight

    for c in loads[:4]:
        c.wait()
    for r in range(0, length, 128):
        ext[8 + r : 8 + r + 128, :] = mult[r : r + 128, :].astype(f32) * value[r : r + 128, :].astype(f32)
    ext_docs[8:, :] = docs[...]
    for c in edges:
        c.wait_recv()
    ext[0:8, :] = (edge_m[...].astype(f32) * edge_v[...].astype(f32))[8:16, :]
    ext_docs[0:8, :] = jnp.where(s > 0, edge_d[...], -1)
    for r in range(0, length, 64):
        now = ext_docs[8 + r : 8 + r + 64, :]
        same = [ext_docs[8 + r - b : 8 + r - b + 64, :] == now for b in range(1, taps_n)]
        for c in range(0, channels, 128):
            acc = taps[taps_n - 1 :, c : c + 128] * ext[8 + r : 8 + r + 64, c : c + 128]
            for b in range(1, taps_n):
                moved = ext[8 + r - b : 8 + r - b + 64, c : c + 128]
                acc = acc + taps[taps_n - 1 - b : taps_n - b, c : c + 128] * jnp.where(same[b - 1], moved, 0.0)
            heads[r : r + 64, c : c + 128] = (gate[r : r + 64, c : c + 128].astype(f32) * acc).astype(bf16)

    loads[4].wait()
    wide = 512

    def projected(number, n):
        return jnp.dot(
            heads[pl.ds(pl.multiple_of(number * count, count), count), :], proj[:, n : n + wide],
            preferred_element_type=f32,
        )

    mix = []
    for i, h in enumerate((1 - hi, hi)):
        for n in range(0, model, wide):
            send1[i, :, n : n + wide] = projected(h * 2 + (1 - lo), n).astype(bf16)
        c = remote(send1.at[i], got1.at[i], mix_s.at[i], mix_r.at[i], tp=sib)
        c.start()
        mix.append(c)
    for n in range(0, model, wide):
        own[:, n : n + wide] = projected((1 - hi) * 2 + lo, n)
    mix[0].wait_recv()
    for n in range(0, model, wide):
        send2[:, n : n + wide] = (own[:, n : n + wide] + got1[0, :, n : n + wide].astype(f32)).astype(bf16)
    c = remote(send2, got2, mix_s.at[2], mix_r.at[2], tp=far)
    c.start()
    mix.append(c)
    for n in range(0, model, wide):
        own[:, n : n + wide] = projected(t, n)
    loads[5].wait()
    mix[1].wait_recv()
    for n in range(0, model, wide):
        q = slice(n, n + wide)
        own[:, q] = own[:, q] + got1[1, :, q].astype(f32) + residual_scale * resid[:, q].astype(f32)
    mix[2].wait_recv()
    for r in range(0, count, 32):
        q = slice(r, r + 32)
        hidden[q, :] = layer_norm(own[q, :] + got2[q, :].astype(f32), gain1[...], bias1[...]).astype(bf16)

    slot_no = lax.broadcasted_iota(jnp.int32, (slots, count), 0).astype(f32)
    mine, other = lo * 2 + hi, lo * 2 + 1 - hi
    pieces = slots // piece

    def selected(e):
        return slot_no == slot_of[pl.ds(e, 1), :]

    def pack(e):
        pick = jnp.where(selected(e), 1.0, 0.0).astype(bf16)
        return jnp.dot(pick, hidden[...], preferred_element_type=f32).astype(bf16)

    def z_out(k, d):
        return remote(packed.at[k, d], rows.at[k, mine, s], zs.at[k, d], zr.at[k, d], sp=(s + d) % experts)

    def x_copy(k):
        block = rows.at[k, mine]
        return remote(block, block, xs.at[k], xr.at[k], tp=far)

    def b_copy(k):
        block = rows.at[k, mine]
        return remote(block, block, bs.at[k], br.at[k], tp=sib)

    def c_copy(k):
        block = rows.at[k, other]
        return remote(block, block, cs.at[k], cr.at[k], tp=sib)

    def r1_copy(k):
        return remote(part.at[k, pl.ds((1 - lo) * 2, 2)], sum_in.at[k], r1s.at[k], r1r.at[k], tp=sib)

    def r2_copy(k):
        return remote(sum_send.at[k], cross_in.at[k], r2s.at[k], r2r.at[k], tp=far)

    def r3_copy(k, d):
        to = (s - d + experts) % experts
        return remote(done_out.at[k, to], back.at[k, s], r3s.at[k, d], r3r.at[k, d], sp=to)

    def each(count_of, run):
        def step(i, _):
            run(i)
            return 0

        lax.fori_loop(0, count_of, step, 0)

    def across(run):
        def step(d, _):
            run(d)
            return 0

        lax.fori_loop(1, experts, step, 0)

    def pack_for(d):
        y = pack((s + d) % experts)
        for k in range(pieces):
            packed[k, d] = y[k * piece : (k + 1) * piece, :]

    across(pack_for)
    each(pieces, lambda k: across(lambda d: z_out(k, d).start()))
    y = pack(s)
    for k in range(pieces):
        rows[k, mine, s] = y[k * piece : (k + 1) * piece, :]

    def pick_for(e):
        pick = jnp.where(selected(e), weight_of[pl.ds(e, 1), :], 0.0)
        high = pick.astype(bf16)
        low = (pick - high.astype(f32)).astype(bf16)
        for k in range(pieces):
            picks[0, k, e] = high[k * piece : (k + 1) * piece, :]
            picks[1, k, e] = low[k * piece : (k + 1) * piece, :]

    each(experts, pick_for)
    for c in loads[6:]:
        c.wait()

    whole = 4 * experts * piece
    group = 4 if whole <= 512 else 1
    size = group * experts * piece

    def experts_of(k):
        def step(m, _):
            block = pl.ds(m * group, group)
            wide_f = 256
            for n in range(0, w_gate.shape[1], wide_f):
                x = rows[k, block].reshape(size, model)
                g = jnp.dot(x, w_gate[:, n : n + wide_f], preferred_element_type=f32)
                u = jnp.dot(x, w_up[:, n : n + wide_f], preferred_element_type=f32)
                hid[:, n : n + wide_f] = (jax.nn.silu(g) * u).astype(bf16)
            for n in range(0, model, wide_f):
                y = jnp.dot(hid[...], w_down[:, n : n + wide_f], preferred_element_type=f32)
                part[k, block, :, :, n : n + wide_f] = y.astype(bf16).reshape(group, experts, piece, wide_f)
            return 0

        lax.fori_loop(0, 4 // group, step, 0)

    def turn(d, _):
        @pl.when(d < pieces)
        def _():
            across(lambda i: z_out(d, i).wait_recv())
            x_copy(d).start()
            b_copy(d).start()

        @pl.when(d >= 3)
        def _():
            k = d - 3
            r2_copy(k).wait_recv()

            def add(j):
                total = part[k, mine, j].astype(f32) + sum_in[k, hi, j].astype(f32) + cross_in[k, j].astype(f32)
                done_out[k, j] = total.astype(bf16)

            each(experts, add)
            across(lambda i: r3_copy(k, i).start())
            back[k, s] = done_out[k, s]

        @pl.when(jnp.logical_and(d >= 2, d < pieces + 2))
        def _():
            k = d - 2
            r1_copy(k).wait_recv()

            def add(j):
                total = part[k, other, j].astype(f32) + sum_in[k, 1 - hi, j].astype(f32)
                sum_send[k, j] = total.astype(bf16)

            each(experts, add)
            r2_copy(k).start()

        @pl.when(jnp.logical_and(d >= 1, d < pieces + 1))
        def _():
            k = d - 1
            x_copy(k).wait_recv()
            c_copy(k).start()
            b_copy(k).wait_recv()
            c_copy(k).wait_recv()
            experts_of(k)
            r1_copy(k).start()

        return 0

    lax.fori_loop(0, pieces + 3, turn, 0)

    each(pieces, lambda k: across(lambda d: r3_copy(k, d).wait_recv()))
    dims = (((0,), (0,)), ((), ()))
    total_slots = pieces * experts * piece
    high = picks[0].reshape(total_slots, count)
    low = picks[1].reshape(total_slots, count)
    for n in range(0, model, 512):
        value_of = back[:, :, :, n : n + 512].reshape(total_slots, 512)
        own[:, n : n + 512] = (
            residual_scale * hidden[:, n : n + 512].astype(f32)
            + lax.dot_general(high, value_of, dims, preferred_element_type=f32)
            + lax.dot_general(low, value_of, dims, preferred_element_type=f32)
        )
    for r in range(0, count, 32):
        q = slice(r, r + 32)
        out[q, :] = layer_norm(own[q, :], gain2[...], bias2[...]).astype(bf16)

    for c in edges + mix:
        c.wait_send()

    def drain(k):
        for c in (x_copy, b_copy, c_copy, r1_copy, r2_copy):
            c(k).wait_send()
        across(lambda d: z_out(k, d).wait_send())
        across(lambda d: r3_copy(k, d).wait_send())

    each(pieces, drain)


def shards(
    gate_in, mult_in, value_in, doc_ids, conv_taps, out_proj, resid, norm1_gain, norm1_bias,
    expert_ids, expert_wts, w_gate, w_up, w_down, norm2_gain, norm2_bias,
):
    experts, parts = lax.axis_size("sp"), lax.axis_size("tp")
    assert parts == 4
    length, channels = mult_in.shape
    count, model = resid.shape
    top = expert_ids.shape[1]
    units = w_gate.shape[2]
    capacity = 5 * count * top // (4 * experts)
    piece = 16
    pieces = -(-capacity // piece)
    slots = pieces * piece
    padded = max(8, experts)
    docs = jnp.broadcast_to(doc_ids[:, None], (length, 128))
    vmem = pl.BlockSpec(memory_space=pltpu.VMEM)
    hbm = pl.BlockSpec(memory_space=pl.ANY)
    V = pltpu.VMEM
    sems = pltpu.SemaphoreType.DMA
    blocks = (pieces, experts, piece, model)
    routed = (pieces, 4, experts, piece, model)
    batch = 4 * experts * piece if 4 * experts * piece <= 512 else experts * piece
    many, each_way = sems((pieces,)), sems((pieces, experts))
    return pl.pallas_call(
        functools.partial(kernel, experts, slots, piece),
        out_shape=jax.ShapeDtypeStruct((count, model), bf16),
        in_specs=[hbm, hbm, hbm, hbm, vmem, hbm, hbm, vmem, vmem, vmem, vmem, hbm, hbm, hbm, vmem, vmem],
        out_specs=vmem,
        scratch_shapes=[
            V((length, channels), bf16), V((length, channels), bf16), V((length, channels), bf16),
            V((length, 128), jnp.int32), V((channels, model), bf16), V((count, model), bf16),
            V((model, units), bf16), V((model, units), bf16), V((units, model), bf16),
            V((16, channels), bf16), V((16, channels), bf16), V((8, 128), jnp.int32),
            V((length + 8, channels), f32), V((length + 8, 128), jnp.int32), V((length, channels), bf16),
            V((2, count, model), bf16), V((2, count, model), bf16), V((count, model), bf16),
            V((count, model), bf16), V((count, model), f32), V((count, model), bf16),
            V((padded, count), f32), V((padded, count), f32),
            V(blocks, bf16), V(routed, bf16), V(routed, bf16), V((batch, units), bf16),
            V((pieces, 2, experts, piece, model), bf16), V(blocks, bf16), V(blocks, bf16), V(blocks, bf16),
            V(blocks, bf16), V((2, pieces, experts, piece, count), bf16),
            sems((9,)), sems((3,)), sems((3,)), sems((3,)), sems((3,)),
            each_way, each_way, many, many, many, many, many, many,
            many, many, many, many, each_way, each_way,
        ],
        compiler_params=pltpu.CompilerParams(
            collective_id=0, has_side_effects=True, vmem_limit_bytes=62 * 2**20
        ),
    )(
        gate_in, mult_in, value_in, docs, conv_taps.astype(f32), out_proj, resid,
        norm1_gain[None], norm1_bias[None], expert_ids.T, expert_wts.T,
        w_gate[0], w_up[0], w_down[0], norm2_gain[None], norm2_bias[None],
    )


def solution(mesh):
    placed = (
        P(("grp", "sp"), "tp"),
        P(("grp", "sp"), "tp"),
        P(("grp", "sp"), "tp"),
        P(("grp", "sp")),
        P(None, "tp"),
        P("tp", None),
        P(("grp", "sp", "tp"), None),
        P(),
        P(),
        P(("grp", "sp", "tp"), None),
        P(("grp", "sp", "tp"), None),
        P("sp", None, "tp"),
        P("sp", None, "tp"),
        P("sp", "tp", None),
        P(),
        P(),
    )
    return jax.shard_map(
        shards, mesh=mesh, in_specs=placed, out_specs=P(("grp", "sp", "tp"), None), check_vma=False
    )
```

profile of v0, /device:TPU:0, one launch (start us, length us, event | category | flops | bytes accessed | tf_op | source)
XLA Modules:
  0.0 113.9 jit_solution(8860221355312109054)
XLA Ops:
  0.0 1.3 %convert_element_type.3.taps = f32[3,384]{1,0:T(4,128)} convert(bf16[3,384]{1,0:T(4,128)(2,1)} %param.20) | non-fusion elementwise | flops 1152 | bytes 6912 | tf_op jit(solution)/shard_map/convert_element_type | solution.py:364
  1.3 1.5 %broadcast_in_dim.18.docs_h = s32[512,128]{1,0:T(8,128)} broadcast(s32[512]{0:T(512)} %param.19), dimensions={0} | broadcast | bytes 264192 | tf_op jit(solution)/shard_map/broadcast_in_dim | solution.py:330
  2.8 109.3 %shard_map.154 = bf16[128,2048]{1,0:T(8,128)(2,1)} custom-call(bf16[512,384]{1,0:T(8,128)(2,1)} %gate_h.1, bf16[512,384]{1,0:T(8,128)(2,1)} %mult_h.1, bf16[512,384]{1,0:T(8,128)(2,1)} %value_h.1, s32[512,128]{1,0:T(8,128)} %broadcast_in_dim.18.docs_h, f32[3,384]{1,0:T(4,128)} %convert_element_type.3.taps, bf16[384,2048]{1,0:T(8,128)(2,1)} %proj_h.1, ...), custom_call_target="tpu_custom_call" | custom-call | tf_op jit(solution)/shard_map/pallas_call | solution.py:339
  112.1 1.9 %copy.18 = bf16[128,2048]{1,0:T(8,128)(2,1)} copy(bf16[128,2048]{1,0:T(8,128)(2,1)} %shard_map.154) | data formatting | bytes 1048576
where the time goes:
time: 114 us
  Pallas kernels  109 us (96%)
  local copies, waits for them, and re-layouts  3.4 us (3%)
  other arithmetic  1.28 us (1%)
    pallas_call x1, Pallas kernels, shards(): pl.pallas_call(functools.partial(kernel, experts, slots, piece), out_shap...  109 us

commit v1 on v0

v1 whole, which is shorter than its diff:
```python
import functools

import jax
import jax.numpy as jnp
from jax import lax
from jax.experimental import pallas as pl
from jax.experimental.pallas import tpu as pltpu
from jax.sharding import PartitionSpec as P

residual_scale = 2.0**0.5
norm_eps = 1e-05
MESH = pl.DeviceIdType.MESH
f32, bf16 = jnp.float32, jnp.bfloat16
CHUNKS = 4


def layer_norm(pre, gain, bias):
    center = pre - jnp.mean(pre, axis=-1, keepdims=True)
    spread = jnp.mean(center * center, axis=-1, keepdims=True)
    return center * lax.rsqrt(spread + norm_eps) * gain + bias


def remote(src, dst, send, recv, **where):
    return pltpu.make_async_remote_copy(
        src_ref=src, dst_ref=dst, send_sem=send, recv_sem=recv, device_id=where, device_id_type=MESH
    )


def kernel(
    experts, slots, piece,
    gate_h, mult_h, value_h, docs_h, taps_h, proj_h, resid_h, gain1_h, bias1_h, ids_h, wts_h,
    w_gate_h, w_up_h, w_down_h, gain2_h, bias2_h,
    out_h,
    gate, mult, value, docs, taps, proj, resid, gain1, bias1, ids, wts, w_gate, w_up, w_down, gain2, bias2,
    edge_m, edge_v, ext, ext_docs, heads,
    send1, got1, send2, got2, own, hidden, out, slot_of, weight_of, onehot, picks_l, picks,
    rows_l, part_l, sum_in_l, sum_send_l, cross_l, done_l,
    packed, rows, part, hid, sum_in, sum_send, cross_in, done_out, back,
    local, outs, edge_s, edge_r, mix_s, mix_r,
    ls, lr, r2ls, r2lr,
    zs, zr, xs, xr, bs, br, cs, cr, r1s, r1r, r2s, r2r, r3s, r3r,
):
    s, t = lax.axis_index("sp"), lax.axis_index("tp")
    hi, lo = t // 2, t % 2
    sib, far = hi * 2 + (1 - lo), (1 - hi) * 2 + lo
    count, model = resid.shape
    length, channels = mult.shape
    taps_n = taps.shape[0]
    top = ids.shape[0]
    others = experts - 1
    pieces = slots // piece

    def load(i, a, b):
        return pltpu.make_async_copy(a, b, local.at[i])

    pairs = [
        (mult_h, mult), (value_h, value), (docs_h, docs.at[:, 128 : 128 + length]), (taps_h, taps), (gate_h, gate),
        (proj_h, proj), (resid_h, resid), (gain1_h, gain1), (bias1_h, bias1), (ids_h, ids), (wts_h, wts),
        (w_gate_h, w_gate), (w_up_h, w_up), (w_down_h, w_down), (gain2_h, gain2), (bias2_h, bias2),
    ]
    loads = [load(i, a, b) for i, (a, b) in enumerate(pairs)]
    for c in loads[:11]:
        c.start()

    barrier = pltpu.get_barrier_semaphore()

    def greet(d, _):
        pl.semaphore_signal(barrier, inc=1, device_id={"sp": (s + d) % experts}, device_id_type=MESH)
        return 0

    lax.fori_loop(1, experts, greet, 0)
    pl.semaphore_signal(barrier, inc=1, device_id={"tp": sib}, device_id_type=MESH)
    pl.semaphore_signal(barrier, inc=1, device_id={"tp": far}, device_id_type=MESH)
    for c in loads[:3]:
        c.wait()
    pl.semaphore_wait(barrier, experts + 1)

    nxt = (s + 1) % experts
    edges = [
        remote(mult.at[pl.ds(length - 16, 16)], edge_m, edge_s.at[0], edge_r.at[0], sp=nxt),
        remote(value.at[pl.ds(length - 16, 16)], edge_v, edge_s.at[1], edge_r.at[1], sp=nxt),
        remote(docs.at[:, pl.ds(length, 128)], docs.at[:, pl.ds(0, 128)], edge_s.at[2], edge_r.at[2], sp=nxt),
    ]

    @pl.when(s < experts - 1)
    def _():
        for c in edges:
            c.start()

    for c in loads[11:]:
        c.start()

    ones = jnp.ones((128, 128), bf16)
    row_no = lax.broadcasted_iota(jnp.int32, (128, 128), 0)
    lane_no = lax.broadcasted_iota(jnp.int32, (128, 128), 1)

    def column(line, shift, height):
        spread = jnp.where(row_no[:height] + shift == lane_no[:height], line.astype(f32), 0.0)
        return jnp.dot(spread.astype(bf16), ones, preferred_element_type=f32)

    for r in range(0, length, 128):
        ext[8 + r : 8 + r + 128, :] = mult[r : r + 128, :].astype(f32) * value[r : r + 128, :].astype(f32)
        ext_docs[8 + r : 8 + r + 128, :] = column(docs[:, 128 + r : 256 + r], 0, 128)
    ext[0:8, :] = jnp.zeros((8, channels), f32)
    ext_docs[0:8, :] = jnp.full((8, 128), -1.0, f32)
    for c in loads[3:5]:
        c.wait()

    def convolve(r, height):
        now = ext_docs[8 + r : 8 + r + height, :]
        same = [ext_docs[8 + r - b : 8 + r - b + height, :] == now for b in range(1, taps_n)]
        for c in range(0, channels, 128):
            tap = taps[:, c : c + 128].astype(f32)
            acc = tap[taps_n - 1 :] * ext[8 + r : 8 + r + height, c : c + 128]
            for b in range(1, taps_n):
                moved = ext[8 + r - b : 8 + r - b + height, c : c + 128]
                acc = acc + tap[taps_n - 1 - b : taps_n - b] * jnp.where(same[b - 1], moved, 0.0)
            heads[r : r + height, c : c + 128] = (gate[r : r + height, c : c + 128].astype(f32) * acc).astype(bf16)

    for r in range(0, length, 64):
        convolve(r, 64)

    @pl.when(s > 0)
    def _():
        for c in edges:
            c.wait_recv()
        ext[0:8, :] = (edge_m[...].astype(f32) * edge_v[...].astype(f32))[8:16, :]
        ext_docs[0:8, :] = column(docs[:, 0:128], 120, 8)
        convolve(0, 16)

    loads[5].wait()
    wide = 512

    def projected(number, n):
        return jnp.dot(
            heads[pl.ds(pl.multiple_of(number * count, count), count), :], proj[:, n : n + wide],
            preferred_element_type=f32,
        )

    step = count // CHUNKS
    near = [
        remote(send1.at[0, pl.ds(j * step, step)], got1.at[0, pl.ds(j * step, step)], mix_s.at[j], mix_r.at[j], tp=sib)
        for j in range(CHUNKS)
    ]
    over = [
        remote(send2.at[pl.ds(j * step, step)], got2.at[pl.ds(j * step, step)], mix_s.at[CHUNKS + j], mix_r.at[CHUNKS + j], tp=far)
        for j in range(CHUNKS)
    ]
    last = remote(send1.at[1], got1.at[1], mix_s.at[2 * CHUNKS], mix_r.at[2 * CHUNKS], tp=sib)
    for n in range(0, model, wide):
        send1[0, :, n : n + wide] = projected((1 - hi) * 2 + (1 - lo), n).astype(bf16)
    for c in near:
        c.start()
    for n in range(0, model, wide):
        own[:, n : n + wide] = projected((1 - hi) * 2 + lo, n)
    for j in range(CHUNKS):
        q = slice(j * step, (j + 1) * step)
        near[j].wait_recv()
        send2[q, :] = (own[q, :] + got1[0, q, :].astype(f32)).astype(bf16)
        over[j].start()
    for n in range(0, model, wide):
        send1[1, :, n : n + wide] = projected(hi * 2 + (1 - lo), n).astype(bf16)
    last.start()
    loads[6].wait()
    for n in range(0, model, wide):
        own[:, n : n + wide] = projected(t, n) + residual_scale * resid[:, n : n + wide].astype(f32)

    for c in loads[7:11]:
        c.wait()
    padded = slot_of.shape[0]
    expert_no = lax.broadcasted_iota(jnp.int32, (padded, count), 0)
    chosen = jnp.zeros((padded, count), f32)
    weight = jnp.zeros((padded, count), f32)
    for k in range(top):
        same = ids[k : k + 1, :] == expert_no
        chosen = chosen + jnp.where(same, 1.0, 0.0)
        weight = weight + jnp.where(same, wts[k : k + 1, :], 0.0)
    before = lax.broadcasted_iota(jnp.int32, (count, count), 0) < lax.broadcasted_iota(
        jnp.int32, (count, count), 1
    )
    rank = jnp.dot(chosen.astype(bf16), jnp.where(before, 1.0, 0.0).astype(bf16), preferred_element_type=f32)
    slot_of[...] = jnp.where(chosen > 0.5, rank, -1.0)
    weight_of[...] = weight
    slot_no = lax.broadcasted_iota(jnp.int32, (slots, count), 0).astype(f32)

    def choose(d, put):
        e = (s + d) % experts
        selected = slot_no == slot_of[pl.ds(e, 1), :]
        onehot[pl.ds(pl.multiple_of(d * slots, 16), slots), :] = jnp.where(selected, 1.0, 0.0).astype(bf16)
        pick = jnp.where(selected, weight_of[pl.ds(e, 1), :], 0.0)
        high = pick.astype(bf16)
        put(high, (pick - high.astype(f32)).astype(bf16))

    def put_local(high, low):
        picks_l[:, 0:count] = high
        picks_l[:, count : 2 * count] = low

    choose(0, put_local)

    def choose_step(d, _):
        def put(high, low):
            for k in range(pieces):
                picks[k, d - 1, :, 0:count] = high[k * piece : (k + 1) * piece, :]
                picks[k, d - 1, :, count : 2 * count] = low[k * piece : (k + 1) * piece, :]

        choose(d, put)
        return 0

    lax.fori_loop(1, experts, choose_step, 0)

    last.wait_recv()
    for n in range(0, model, wide):
        own[:, n : n + wide] = own[:, n : n + wide] + got1[1, :, n : n + wide].astype(f32)
    for j in range(CHUNKS):
        over[j].wait_recv()
        q = slice(j * step, (j + 1) * step)
        hidden[q, :] = layer_norm(own[q, :] + got2[q, :].astype(f32), gain1[...], bias1[...]).astype(bf16)

    mine, other = lo * 2 + hi, lo * 2 + 1 - hi

    def z_out(k, d):
        return remote(packed.at[k, d - 1], rows.at[k, mine, d - 1], zs.at[k, d - 1], zr.at[k, d - 1], sp=(s + d) % experts)

    def x_copy(k):
        block = rows.at[k, mine]
        return remote(block, block, xs.at[k], xr.at[k], tp=far)

    def b_copy(k):
        block = rows.at[k, mine]
        return remote(block, block, bs.at[k], br.at[k], tp=sib)

    def c_copy(k):
        block = rows.at[k, other]
        return remote(block, block, cs.at[k], cr.at[k], tp=sib)

    def r1_copy(k):
        return remote(part.at[k, pl.ds((1 - lo) * 2, 2)], sum_in.at[k], r1s.at[k], r1r.at[k], tp=sib)

    def r2_copy(k):
        return remote(sum_send.at[k], cross_in.at[k], r2s.at[k], r2r.at[k], tp=far)

    def r3_copy(k, d):
        return remote(done_out.at[k, d - 1], back.at[k, d - 1], r3s.at[k, d - 1], r3r.at[k, d - 1], sp=(s - d + experts) % experts)

    x_l = remote(rows_l.at[mine], rows_l.at[mine], ls.at[0], lr.at[0], tp=far)
    b_l = remote(rows_l.at[mine], rows_l.at[mine], ls.at[1], lr.at[1], tp=sib)
    c_l = remote(rows_l.at[other], rows_l.at[other], ls.at[2], lr.at[2], tp=sib)
    r1_l = remote(part_l.at[pl.ds((1 - lo) * 2, 2)], sum_in_l, ls.at[3], lr.at[3], tp=sib)

    def r2_l(j):
        q = pl.ds(j * piece, piece)
        return remote(sum_send_l.at[q], cross_l.at[q], r2ls.at[j], r2lr.at[j], tp=far)

    def each(count_of, run):
        def step(i, _):
            run(i)
            return 0

        lax.fori_loop(0, count_of, step, 0)

    def across(run):
        def step(d, _):
            run(d)
            return 0

        lax.fori_loop(1, experts, step, 0)

    for n in range(0, model, wide):
        y = jnp.dot(onehot[0:slots, :], hidden[:, n : n + wide], preferred_element_type=f32)
        rows_l[mine, :, n : n + wide] = y.astype(bf16)
    x_l.start()
    b_l.start()
    for n in range(0, model, wide):
        y = jnp.dot(onehot[slots:, :], hidden[:, n : n + wide], preferred_element_type=f32).astype(bf16)
        for d in range(others):
            for k in range(pieces):
                r = d * slots + k * piece
                packed[k, d, :, n : n + wide] = y[r : r + piece, :]
    each(pieces, lambda k: across(lambda d: z_out(k, d).start()))
    for n in range(0, model, wide):
        own[:, n : n + wide] = residual_scale * hidden[:, n : n + wide].astype(f32)
    for c in loads[11:]:
        c.wait()

    wide_f = 256

    def ffn(size, take, put):
        for n in range(0, w_gate.shape[1], wide_f):
            x = take()
            g = jnp.dot(x, w_gate[:, n : n + wide_f], preferred_element_type=f32)
            u = jnp.dot(x, w_up[:, n : n + wide_f], preferred_element_type=f32)
            hid[0:size, n : n + wide_f] = (jax.nn.silu(g) * u).astype(bf16)
        for n in range(0, model, wide_f):
            y = jnp.dot(hid[0:size, :], w_down[:, n : n + wide_f], preferred_element_type=f32)
            put(n, y.astype(bf16))

    group = 4 if 4 * others * piece <= 512 else 1
    size = group * others * piece

    def experts_of(k):
        def run(m, _):
            block = pl.ds(m * group, group)

            def put(n, y):
                part[k, block, :, :, n : n + wide_f] = y.reshape(group, others, piece, wide_f)

            ffn(size, lambda: rows[k, block].reshape(size, model), put)
            return 0

        if group == 4:
            run(0, 0)
        else:
            lax.fori_loop(0, 4 // group, run, 0)

    def put_l(n, y):
        part_l[:, :, n : n + wide_f] = y.reshape(4, slots, wide_f)

    def arrive(k):
        across(lambda d: z_out(k, d).wait_recv())
        x_copy(k).start()
        b_copy(k).start()

    def combine(pick, value_of):
        dims = (((0,), (0,)), ((), ()))
        for n in range(0, model, wide):
            y = lax.dot_general(pick, value_of(n), dims, preferred_element_type=f32)
            own[:, n : n + wide] = own[:, n : n + wide] + y[0:count, :] + y[count:, :]

    def give_back(k):
        across(lambda d: r3_copy(k, d).wait_recv())
        combine(
            picks[k].reshape(others * piece, 2 * count),
            lambda n: back[k, :, :, n : n + wide].reshape(others * piece, wide),
        )

    arrive(0)
    x_l.wait_recv()
    c_l.start()
    b_l.wait_recv()
    c_l.wait_recv()
    ffn(4 * slots, lambda: rows_l[...].reshape(4 * slots, model), put_l)
    r1_l.start()

    def turn(d, _):
        @pl.when(d < pieces)
        def _():
            arrive(d)

        @pl.when(d == 1)
        def _():
            r1_l.wait_recv()

            def add(j):
                q = pl.ds(pl.multiple_of(j * piece, 16), piece)
                sum_send_l[q, :] = (part_l[other, q, :].astype(f32) + sum_in_l[1 - hi, q, :].astype(f32)).astype(bf16)

            each(pieces, add)

        @pl.when(jnp.logical_and(d >= 2, d < pieces + 2))
        def _():
            k = d - 2
            r1_copy(k).wait_recv()

            def add(j):
                total = part[k, other, j].astype(f32) + sum_in[k, 1 - hi, j].astype(f32)
                sum_send[k, j] = total.astype(bf16)

            each(others, add)
            r2_copy(k).start()

        @pl.when(d == pieces + 1)
        def _():
            each(pieces, lambda j: r2_l(j).start())

        @pl.when(d < pieces + 1)
        def _():
            k = d - 1
            x_copy(k).wait_recv()
            c_copy(k).start()
            b_copy(k).wait_recv()
            c_copy(k).wait_recv()
            experts_of(k)
            r1_copy(k).start()

        @pl.when(d >= 3)
        def _():
            k = d - 3
            r2_copy(k).wait_recv()

            def add(j):
                total = part[k, mine, j].astype(f32) + sum_in[k, hi, j].astype(f32) + cross_in[k, j].astype(f32)
                done_out[k, j] = total.astype(bf16)

            each(others, add)
            across(lambda i: r3_copy(k, i).start())

        return 0

    lax.fori_loop(1, pieces + 3, turn, 0)
    for k in range(max(pieces - 2, 0)):
        give_back(k)

    def add_l(j):
        q = pl.ds(pl.multiple_of(j * piece, 16), piece)
        r2_l(j).wait_recv()
        total = part_l[mine, q, :].astype(f32) + sum_in_l[hi, q, :].astype(f32) + cross_l[q, :].astype(f32)
        done_l[q, :] = total.astype(bf16)

    each(pieces, add_l)
    combine(picks_l[...], lambda n: done_l[:, n : n + wide])
    for k in range(max(pieces - 2, 0), pieces):
        give_back(k)

    finals = []
    for j in range(CHUNKS):
        q = slice(j * step, (j + 1) * step)
        out[q, :] = layer_norm(own[q, :], gain2[...], bias2[...]).astype(bf16)
        c = pltpu.make_async_copy(out.at[pl.ds(j * step, step)], out_h.at[pl.ds(j * step, step)], outs.at[j])
        c.start()
        finals.append(c)

    @pl.when(s < experts - 1)
    def _():
        for c in edges:
            c.wait_send()

    for c in near + over + [last, x_l, b_l, c_l, r1_l]:
        c.wait_send()

    def drain(k):
        for c in (x_copy, b_copy, c_copy, r1_copy, r2_copy, r2_l):
            c(k).wait_send()
        across(lambda d: z_out(k, d).wait_send())
        across(lambda d: r3_copy(k, d).wait_send())

    each(pieces, drain)
    for c in finals:
        c.wait()


def shards(
    gate_in, mult_in, value_in, doc_ids, conv_taps, out_proj, resid, norm1_gain, norm1_bias,
    expert_ids, expert_wts, w_gate, w_up, w_down, norm2_gain, norm2_bias,
):
    experts, parts = lax.axis_size("sp"), lax.axis_size("tp")
    assert parts == 4
    length, channels = mult_in.shape
    count, model = resid.shape
    top = expert_ids.shape[1]
    units = w_gate.shape[2]
    capacity = 5 * count * top // (4 * experts)
    piece = 16
    pieces = -(-capacity // piece)
    slots = pieces * piece
    padded = max(8, experts)
    others = experts - 1
    hbm = pl.BlockSpec(memory_space=pl.ANY)
    V = pltpu.VMEM
    sems = pltpu.SemaphoreType.DMA
    blocks = (pieces, others, piece, model)
    routed = (pieces, 4, others, piece, model)
    batch = 4 * others * piece if 4 * others * piece <= 512 else others * piece
    batch = max(batch, 4 * slots)
    many, each_way = sems((pieces,)), sems((pieces, others))
    return pl.pallas_call(
        functools.partial(kernel, experts, slots, piece),
        out_shape=jax.ShapeDtypeStruct((count, model), bf16),
        in_specs=[hbm] * 16,
        out_specs=hbm,
        scratch_shapes=[
            V((length, channels), bf16), V((length, channels), bf16), V((length, channels), bf16),
            V((1, length + 128), jnp.int32), V(conv_taps.shape, bf16), V((channels, model), bf16), V((count, model), bf16),
            V((1, model), f32), V((1, model), f32), V((top, count), jnp.int32), V((top, count), f32),
            V((model, units), bf16), V((model, units), bf16), V((units, model), bf16), V((1, model), f32), V((1, model), f32),
            V((16, channels), bf16), V((16, channels), bf16),
            V((length + 8, channels), f32), V((length + 8, 128), f32), V((length, channels), bf16),
            V((2, count, model), bf16), V((2, count, model), bf16), V((count, model), bf16),
            V((count, model), bf16), V((count, model), f32), V((count, model), bf16), V((count, model), bf16),
            V((padded, count), f32), V((padded, count), f32), V((experts * slots, count), bf16),
            V((slots, 2 * count), bf16), V((pieces, others, piece, 2 * count), bf16),
            V((4, slots, model), bf16), V((4, slots, model), bf16), V((2, slots, model), bf16),
            V((slots, model), bf16), V((slots, model), bf16), V((slots, model), bf16),
            V(blocks, bf16), V(routed, bf16), V(routed, bf16), V((batch, units), bf16),
            V((pieces, 2, others, piece, model), bf16), V(blocks, bf16), V(blocks, bf16), V(blocks, bf16),
            V(blocks, bf16),
            sems((16,)), sems((CHUNKS,)), sems((3,)), sems((3,)), sems((2 * CHUNKS + 1,)), sems((2 * CHUNKS + 1,)),
            sems((4,)), sems((4,)), many, many,
            each_way, each_way, many, many, many, many, many, many,
            many, many, many, many, each_way, each_way,
        ],
        compiler_params=pltpu.CompilerParams(
            collective_id=0, has_side_effects=True, vmem_limit_bytes=62 * 2**20
        ),
    )(
        gate_in, mult_in, value_in, doc_ids[None], conv_taps, out_proj, resid,
        norm1_gain[None], norm1_bias[None], expert_ids.T, expert_wts.T,
        w_gate[0], w_up[0], w_down[0], norm2_gain[None], norm2_bias[None],
    )


def solution(mesh):
    placed = (
        P(("grp", "sp"), "tp"),
        P(("grp", "sp"), "tp"),
        P(("grp", "sp"), "tp"),
        P(("grp", "sp")),
        P(None, "tp"),
        P("tp", None),
        P(("grp", "sp", "tp"), None),
        P(),
        P(),
        P(("grp", "sp", "tp"), None),
        P(("grp", "sp", "tp"), None),
        P("sp", None, "tp"),
        P("sp", None, "tp"),
        P("sp", "tp", None),
        P(),
        P(),
    )
    return jax.shard_map(
        shards, mesh=mesh, in_specs=placed, out_specs=P(("grp", "sp", "tp"), None), check_vma=False
    )
```

time: 114 us -> 98.3 us (0.86)
  Pallas kernels: 109 us -> 96.2 us
  local copies, waits for them, and re-layouts: 3.4 us -> 1.88 us
  other arithmetic: 1.28 us -> 0 us
    pallas_call x1, Pallas kernels: 109 us -> 96.2 us  [shards(): pl.pallas_call(functools.partial(kernel, experts, slots, piece), out_shap...]
    broadcast_in_dim x1 -> x0, local copies, waits for them, and re-layouts: 1.52 us -> none  [shards(): docs = jnp.broadcast_to(doc_ids[:, None], (length, 128))]
    convert_element_type x1 -> x0, other arithmetic: 1.28 us -> none  [shards(): conv_taps.astype(f32)]
where the time goes in v1:
time: 98.3 us; the launch traced here: 98.1 us
  Pallas kernels  96.2 us (98%)
  local copies, waits for them, and re-layouts  1.88 us (2%)
    pallas_call x1, Pallas kernels, shards(): pl.pallas_call(functools.partial(kernel, experts, slots, piece), out_shap...  96.2 us

profile of v1, /device:TPU:0, one launch (start us, length us, event | category | flops | bytes accessed | tf_op | source)
XLA Modules:
  0.0 98.1 jit_solution(13805571339146178661)
XLA Ops:
  0.0 96.2 %shard_map.154 = bf16[128,2048]{1,0:T(8,128)(2,1)} custom-call(bf16[512,384]{1,0:T(8,128)(2,1)} %gate_h.1, bf16[512,384]{1,0:T(8,128)(2,1)} %mult_h.1, bf16[512,384]{1,0:T(8,128)(2,1)} %value_h.1, s32[1,512]{1,0:T(1,128)} %bitcast.17, bf16[3,384]{1,0:T(4,128)(2,1)} %taps_h.1, bf16[384,2048]{1,0:T(8,128)(2,1)} %proj_h.1, bf16[128,2048]{1,0:T(8,128)(2,1)} %resid_h.1, ...), custom_call_target="tpu_custom_call" | custom-call | tf_op jit(solution)/shard_map/pallas_call | solution.py:465
  96.2 1.9 %copy.18 = bf16[128,2048]{1,0:T(8,128)(2,1)} copy(bf16[128,2048]{1,0:T(8,128)(2,1)} %shard_map.154) | data formatting | bytes 1048576

commit v2 on v1

v2 whole, which is shorter than its diff:
```python
import functools

import jax
import jax.numpy as jnp
from jax import lax
from jax.experimental import pallas as pl
from jax.experimental.pallas import tpu as pltpu
from jax.sharding import PartitionSpec as P

residual_scale = 2.0**0.5
norm_eps = 1e-05
MESH = pl.DeviceIdType.MESH
f32, bf16 = jnp.float32, jnp.bfloat16
CHUNKS = 4


def layer_norm(pre, gain, bias):
    center = pre - jnp.mean(pre, axis=-1, keepdims=True)
    spread = jnp.mean(center * center, axis=-1, keepdims=True)
    return center * lax.rsqrt(spread + norm_eps) * gain + bias


def remote(src, dst, send, recv, **where):
    return pltpu.make_async_remote_copy(
        src_ref=src, dst_ref=dst, send_sem=send, recv_sem=recv, device_id=where, device_id_type=MESH
    )


def kernel(
    experts, slots, piece,
    gate_h, mult_h, value_h, docs_h, taps_h, proj_h, resid_h, gain1_h, bias1_h, ids_h, wts_h,
    w_gate_h, w_up_h, w_down_h, gain2_h, bias2_h,
    out_h,
    gate, mult, value, docs, taps, proj, resid, gain1, bias1, ids, wts, w_gate, w_up, w_down, gain2, bias2,
    edge_m, edge_v, ext, ext_docs, heads,
    send1, got1, send2, got2, own, hidden, hidden_far, out, ids_far, wts_far,
    slot_of, weight_of, onehot_n, onehot, picks_n, picks,
    rows_n, part_n, pack_n, sum_in_n, total_n, near_back, dense_send, dense_in,
    packed, rows, part, hid, sum_in, sum_send, cross_in, done_out, back,
    local, outs, edge_s, edge_r, mix_s, mix_r, swap_s, swap_r, dense_s, dense_r,
    lbs, lbr, ns, nr, nbs, nbr, n1s, n1r, rns, rnr, des, der,
    zs, zr, xs, xr, bs, br, cs, cr, r1s, r1r, r2s, r2r, r3s, r3r,
):
    s, t = lax.axis_index("sp"), lax.axis_index("tp")
    hi, lo = t // 2, t % 2
    sib, far = hi * 2 + (1 - lo), (1 - hi) * 2 + lo
    count, model = resid.shape
    length, channels = mult.shape
    taps_n = taps.shape[0]
    top = ids.shape[0]
    others = experts - 2
    pieces = slots // piece
    parity = s % 2
    base = s - parity
    near = base + 1 - parity

    def load(i, a, b):
        return pltpu.make_async_copy(a, b, local.at[i])

    pairs = [
        (mult_h, mult), (value_h, value), (docs_h, docs.at[:, 128 : 128 + length]), (taps_h, taps), (gate_h, gate),
        (proj_h, proj), (resid_h, resid), (gain1_h, gain1), (bias1_h, bias1), (ids_h, ids), (wts_h, wts),
        (w_gate_h, w_gate), (w_up_h, w_up), (w_down_h, w_down), (gain2_h, gain2), (bias2_h, bias2),
    ]
    loads = [load(i, a, b) for i, (a, b) in enumerate(pairs)]
    for c in loads[:11]:
        c.start()

    barrier = pltpu.get_barrier_semaphore()

    def greet(d, _):
        pl.semaphore_signal(barrier, inc=1, device_id={"sp": (s + d) % experts}, device_id_type=MESH)
        return 0

    lax.fori_loop(1, experts, greet, 0)
    pl.semaphore_signal(barrier, inc=1, device_id={"tp": sib}, device_id_type=MESH)
    pl.semaphore_signal(barrier, inc=1, device_id={"tp": far}, device_id_type=MESH)
    for c in loads[:3]:
        c.wait()
    pl.semaphore_wait(barrier, experts + 1)

    nxt = (s + 1) % experts
    edges = [
        remote(mult.at[pl.ds(length - 16, 16)], edge_m, edge_s.at[0], edge_r.at[0], sp=nxt),
        remote(value.at[pl.ds(length - 16, 16)], edge_v, edge_s.at[1], edge_r.at[1], sp=nxt),
        remote(docs.at[:, pl.ds(length, 128)], docs.at[:, pl.ds(0, 128)], edge_s.at[2], edge_r.at[2], sp=nxt),
    ]

    @pl.when(s < experts - 1)
    def _():
        for c in edges:
            c.start()

    for c in loads[11:]:
        c.start()

    ones = jnp.ones((128, 128), bf16)
    row_no = lax.broadcasted_iota(jnp.int32, (128, 128), 0)
    lane_no = lax.broadcasted_iota(jnp.int32, (128, 128), 1)

    def column(line, shift, height):
        spread = jnp.where(row_no[:height] + shift == lane_no[:height], line.astype(f32), 0.0)
        return jnp.dot(spread.astype(bf16), ones, preferred_element_type=f32)

    for r in range(0, length, 128):
        ext[8 + r : 8 + r + 128, :] = mult[r : r + 128, :].astype(f32) * value[r : r + 128, :].astype(f32)
        ext_docs[8 + r : 8 + r + 128, :] = column(docs[:, 128 + r : 256 + r], 0, 128)
    ext[0:8, :] = jnp.zeros((8, channels), f32)
    ext_docs[0:8, :] = jnp.full((8, 128), -1.0, f32)
    for c in loads[3:5]:
        c.wait()

    def convolve(r, height):
        now = ext_docs[8 + r : 8 + r + height, :]
        same = [ext_docs[8 + r - b : 8 + r - b + height, :] == now for b in range(1, taps_n)]
        for c in range(0, channels, 128):
            tap = taps[:, c : c + 128].astype(f32)
            acc = tap[taps_n - 1 :] * ext[8 + r : 8 + r + height, c : c + 128]
            for b in range(1, taps_n):
                moved = ext[8 + r - b : 8 + r - b + height, c : c + 128]
                acc = acc + tap[taps_n - 1 - b : taps_n - b] * jnp.where(same[b - 1], moved, 0.0)
            heads[r : r + height, c : c + 128] = (gate[r : r + height, c : c + 128].astype(f32) * acc).astype(bf16)

    for r in range(0, length, 64):
        convolve(r, 64)

    @pl.when(s > 0)
    def _():
        for c in edges:
            c.wait_recv()
        ext[0:8, :] = (edge_m[...].astype(f32) * edge_v[...].astype(f32))[8:16, :]
        ext_docs[0:8, :] = column(docs[:, 0:128], 120, 8)
        convolve(0, 16)

    for c in loads[7:11]:
        c.wait()
    swaps = [
        remote(ids, ids_far, swap_s.at[0], swap_r.at[0], tp=far),
        remote(wts, wts_far, swap_s.at[1], swap_r.at[1], tp=far),
    ]
    for c in swaps:
        c.start()
    loads[5].wait()
    wide = 512

    def projected(number, n):
        return jnp.dot(
            heads[pl.ds(pl.multiple_of(number * count, count), count), :], proj[:, n : n + wide],
            preferred_element_type=f32,
        )

    step = count // CHUNKS
    beside = [
        remote(send1.at[0, pl.ds(j * step, step)], got1.at[0, pl.ds(j * step, step)], mix_s.at[j], mix_r.at[j], tp=sib)
        for j in range(CHUNKS)
    ]
    over = [
        remote(send2.at[pl.ds(j * step, step)], got2.at[pl.ds(j * step, step)], mix_s.at[CHUNKS + j], mix_r.at[CHUNKS + j], tp=far)
        for j in range(CHUNKS)
    ]
    last = remote(send1.at[1], got1.at[1], mix_s.at[2 * CHUNKS], mix_r.at[2 * CHUNKS], tp=sib)
    dense = [
        remote(hidden.at[pl.ds(j * step, step)], hidden_far.at[pl.ds(j * step, step)], dense_s.at[j], dense_r.at[j], tp=far)
        for j in range(CHUNKS)
    ]
    for n in range(0, model, wide):
        send1[0, :, n : n + wide] = projected((1 - hi) * 2 + (1 - lo), n).astype(bf16)
    for c in beside:
        c.start()
    for n in range(0, model, wide):
        own[:, n : n + wide] = projected((1 - hi) * 2 + lo, n)
    for j in range(CHUNKS):
        q = slice(j * step, (j + 1) * step)
        beside[j].wait_recv()
        send2[q, :] = (own[q, :] + got1[0, q, :].astype(f32)).astype(bf16)
        over[j].start()
    for n in range(0, model, wide):
        send1[1, :, n : n + wide] = projected(hi * 2 + (1 - lo), n).astype(bf16)
    last.start()
    loads[6].wait()
    for n in range(0, model, wide):
        own[:, n : n + wide] = projected(t, n) + residual_scale * resid[:, n : n + wide].astype(f32)
    last.wait_recv()
    for n in range(0, model, wide):
        own[:, n : n + wide] = own[:, n : n + wide] + got1[1, :, n : n + wide].astype(f32)

    padded = slot_of.shape[1]
    expert_no = lax.broadcasted_iota(jnp.int32, (padded, count), 0)
    token_no = lax.broadcasted_iota(jnp.int32, (padded, count), 1)
    before = lax.broadcasted_iota(jnp.int32, (count, count), 0) < lax.broadcasted_iota(
        jnp.int32, (count, count), 1
    )
    slot_no = lax.broadcasted_iota(jnp.int32, (slots, count), 0).astype(f32)
    ready = [max(0, slots - (count - (j + 1) * step)) // piece for j in range(CHUNKS)]

    def choose(side, e, put):
        selected = slot_no == slot_of[side, pl.ds(e, 1), :]
        pick = jnp.where(selected, weight_of[side, pl.ds(e, 1), :], 0.0)
        high = pick.astype(bf16)
        put(jnp.where(selected, 1.0, 0.0).astype(bf16), high, (pick - high.astype(f32)).astype(bf16))

    def route(side, own_side, its_ids, its_wts):
        chosen = jnp.zeros((padded, count), f32)
        weight = jnp.zeros((padded, count), f32)
        for k in range(top):
            same = its_ids[k : k + 1, :] == expert_no
            chosen = chosen + jnp.where(same, 1.0, 0.0)
            weight = weight + jnp.where(same, its_wts[k : k + 1, :], 0.0)
        rank = jnp.dot(chosen.astype(bf16), jnp.where(before, 1.0, 0.0).astype(bf16), preferred_element_type=f32)
        slot, placed, open_ = jnp.full((padded, count), -1.0, f32), jnp.zeros((padded, 1), f32), 0
        for j in range(CHUNKS):
            seen = jnp.where(token_no < (j + 1) * step, chosen, 0.0)
            upto = jnp.minimum(jnp.sum(seen, axis=1, keepdims=True), placed + float(ready[j] * piece - open_))
            here = jnp.logical_and(rank >= placed, rank < upto)
            slot = jnp.where(here, rank - placed + float(open_), slot)
            placed, open_ = upto, ready[j] * piece
        slot_of[side] = jnp.where(chosen > 0.5, slot, -1.0)
        weight_of[side] = weight
        for n, e in enumerate((s, near)):
            def put(one, high, low):
                if own_side:
                    for k in range(pieces):
                        onehot[k, others + n] = one[k * piece : (k + 1) * piece, :]
                else:
                    onehot_n[n * slots : (n + 1) * slots, :] = one
                picks_n[side, n * slots : (n + 1) * slots, 0:count] = high
                picks_n[side, n * slots : (n + 1) * slots, count : 2 * count] = low

            choose(side, e, put)

    route(hi, True, ids, wts)

    def choose_step(i, _):
        def put(one, high, low):
            for k in range(pieces):
                onehot[k, i] = one[k * piece : (k + 1) * piece, :]
                picks[k, i, :, 0:count] = high[k * piece : (k + 1) * piece, :]
                picks[k, i, :, count : 2 * count] = low[k * piece : (k + 1) * piece, :]

        choose(hi, (base + 2 + i) % experts, put)
        return 0

    lax.fori_loop(0, others, choose_step, 0)
    for c in swaps:
        c.wait_recv()
    route(1 - hi, False, ids_far, wts_far)

    hidden[...] = jnp.zeros((count, model), bf16)

    mine, other = lo * 2 + hi, lo * 2 + 1 - hi

    def z_out(k, i):
        j = 2 * (i // 2) + parity
        return remote(packed.at[k, i], rows.at[k, mine, j], zs.at[k, i], zr.at[k, j], sp=(base + 2 + i) % experts)

    def z_got(k, j):
        return remote(packed.at[k, j], rows.at[k, mine, j], zs.at[k, j], zr.at[k, j], sp=near)

    def x_copy(k):
        block = rows.at[k, mine]
        return remote(block, block, xs.at[k], xr.at[k], tp=far)

    def b_copy(k):
        block = rows.at[k, mine]
        return remote(block, block, bs.at[k], br.at[k], tp=sib)

    def c_copy(k):
        block = rows.at[k, other]
        return remote(block, block, cs.at[k], cr.at[k], tp=sib)

    def r1_copy(k):
        return remote(part.at[k, pl.ds((1 - lo) * 2, 2)], sum_in.at[k], r1s.at[k], r1r.at[k], tp=sib)

    def r2_copy(k):
        return remote(sum_send.at[k], cross_in.at[k], r2s.at[k], r2r.at[k], tp=far)

    def r3_copy(k, j):
        i = 2 * (j // 2) + parity
        to = (base - 2 - 2 * (j // 2) + j % 2 + experts) % experts
        return remote(done_out.at[k, j], back.at[k, i], r3s.at[k, j], r3r.at[k, i], sp=to)

    def r3_got(k, i):
        return remote(done_out.at[k, i], back.at[k, i], r3s.at[k, i], r3r.at[k, i], sp=near)

    def local_copy(h):
        block = rows_n.at[0, h, lo]
        return remote(block, block, lbs.at[h], lbr.at[h], tp=sib)

    def near_far():
        return remote(pack_n.at[1 - hi], rows_n.at[1, 1 - hi, lo], ns.at[CHUNKS], nr.at[CHUNKS], sp=near)

    def near_own(j, first, stop):
        q = pl.ds(first * piece, (stop - first) * piece)
        return remote(pack_n.at[hi, q], rows_n.at[1, hi, lo, q], ns.at[j], nr.at[j], sp=near)

    stages, begun = [], 0
    for j in range(CHUNKS):
        if ready[j] > begun:
            stages.append((j, begun, ready[j]))
            begun = ready[j]
    held = max(pieces - 2, 1)

    def near_share(h):
        block = rows_n.at[1, h, lo]
        return remote(block, block, nbs.at[h], nbr.at[h], tp=sib)

    def near_sum(n, h):
        return remote(part_n.at[n, h, 1 - lo], sum_in_n.at[n, h], n1s.at[n, h], n1r.at[n, h], tp=sib)

    def near_return(h, c):
        return remote(total_n.at[h, c], near_back.at[h, c, 1], rns.at[h, c], rnr.at[h, c], sp=near)

    def dense_copy(c):
        return remote(dense_send.at[c], dense_in.at[c], des.at[c], der.at[c], tp=far)

    def each(count_of, run):
        def step(i, _):
            run(i)
            return 0

        lax.fori_loop(0, count_of, step, 0)

    def across(run):
        each(others, run)

    for j in range(CHUNKS):
        over[j].wait_recv()
        q = slice(j * step, (j + 1) * step)
        hidden[q, :] = layer_norm(own[q, :] + got2[q, :].astype(f32), gain1[...], bias1[...]).astype(bf16)
        dense[j].start()
        for number, first, stop in stages:
            if number != j:
                continue
            span = stop - first
            q = slice(first * piece, stop * piece)
            for n in range(0, model, wide):
                y = jnp.dot(
                    onehot[first:stop].reshape(span * experts * piece, count), hidden[:, n : n + wide],
                    preferred_element_type=f32,
                ).astype(bf16).reshape(span, experts, piece, wide)
                packed[first:stop, :, :, n : n + wide] = y[:, :others]
                rows_n[0, hi, lo, q, n : n + wide] = y[:, others].reshape(span * piece, wide)
                pack_n[hi, q, n : n + wide] = y[:, others + 1].reshape(span * piece, wide)
            near_own(j, first, stop).start()
            for k in range(first, min(stop, held)):
                across(lambda i: z_out(k, i).start())

    local_copy(hi).start()
    for n in range(0, model, wide):
        own[:, n : n + wide] = residual_scale * hidden[:, n : n + wide].astype(f32)
    for c in loads[11:]:
        c.wait()

    wide_f = 256

    def ffn(size, take, put):
        for n in range(0, w_gate.shape[1], wide_f):
            x = take()
            g = jnp.dot(x, w_gate[:, n : n + wide_f], preferred_element_type=f32)
            u = jnp.dot(x, w_up[:, n : n + wide_f], preferred_element_type=f32)
            hid[0:size, n : n + wide_f] = (jax.nn.silu(g) * u).astype(bf16)
        for n in range(0, model, wide_f):
            y = jnp.dot(hid[0:size, :], w_down[:, n : n + wide_f], preferred_element_type=f32)
            put(n, y.astype(bf16))

    group = 4 if 4 * others * piece <= 512 else 1
    size = group * others * piece

    def experts_of(k):
        def run(m, _):
            block = pl.ds(m * group, group)

            def put(n, y):
                part[k, block, :, :, n : n + wide_f] = y.reshape(group, others, piece, wide_f)

            ffn(size, lambda: rows[k, block].reshape(size, model), put)
            return 0

        if group == 4:
            run(0, 0)
        else:
            lax.fori_loop(0, 4 // group, run, 0)

    def arrive(k):
        across(lambda j: z_got(k, j).wait_recv())
        x_copy(k).start()
        b_copy(k).start()

    half = model // 2

    def near_total(n, h, put):
        near_sum(n, h).wait_recv()
        for c in range(2):
            q = slice(c * half, (c + 1) * half)
            total = part_n[n, h, lo, :, q].astype(f32) + sum_in_n[n, h, :, q].astype(f32)
            put(c, total.astype(bf16))

    def near_expert(h):
        near_share(h).wait_recv()

        def put(n, y):
            part_n[1, h, :, :, n : n + wide_f] = y.reshape(2, slots, wide_f)

        ffn(2 * slots, lambda: rows_n[1, h].reshape(2 * slots, model), put)
        near_sum(1, h).start()

    def near_home(h):
        def put(c, y):
            total_n[h, c] = y
            near_return(h, c).start()

        near_total(1, h, put)

    dims = (((0,), (0,)), ((), ()))

    def near_combine(h, c, put):
        near_return(h, c).wait_recv()
        for n in range(0, half, wide):
            y = lax.dot_general(
                picks_n[h], near_back[h, c, :, :, n : n + wide].reshape(2 * slots, wide), dims, preferred_element_type=f32
            )
            put(n, y[0:count, :] + y[count:, :])

    def far_combine(c):
        def put(n, y):
            dense_send[c, :, n : n + wide] = y.astype(bf16)

        near_combine(1 - hi, c, put)
        dense_copy(c).start()

    def give_back(k):
        across(lambda i: r3_got(k, i).wait_recv())
        for n in range(0, model, wide):
            y = lax.dot_general(
                picks[k].reshape(others * piece, 2 * count), back[k, :, :, n : n + wide].reshape(others * piece, wide),
                dims, preferred_element_type=f32,
            )
            own[:, n : n + wide] = own[:, n : n + wide] + y[0:count, :] + y[count:, :]

    arrive(0)
    for c in dense:
        c.wait_recv()
    for n in range(0, model, wide):
        y = jnp.dot(onehot_n[...], hidden_far[:, n : n + wide], preferred_element_type=f32).astype(bf16)
        rows_n[0, 1 - hi, lo, :, n : n + wide] = y[0:slots, :]
        pack_n[1 - hi, :, n : n + wide] = y[slots:, :]
    near_far().start()
    for k in range(held, pieces):
        across(lambda i: z_out(k, i).start())
    local_copy(1 - hi).start()
    if pieces > 1:
        arrive(1)

    def put_local(n, y):
        part_n[0, :, :, :, n : n + wide_f] = y.reshape(2, 2, slots, wide_f)

    def local_expert():
        local_copy(hi).wait_recv()
        local_copy(1 - hi).wait_recv()
        ffn(4 * slots, lambda: rows_n[0].reshape(4 * slots, model), put_local)
        near_sum(0, 0).start()
        near_sum(0, 1).start()

    steps = {"share": 3, "expert": 3, "home": 4, "local": 4, "total": 5, "expert_own": 5, "home_own": 6, "cross": 6, "cross2": 6}
    turns = max(pieces + 3, max(steps.values()) + 1)

    def turn(d, _):
        def at(name, run):
            @pl.when(d == steps[name])
            def _():
                run()

        @pl.when(d < pieces + 1)
        def _():
            k = d - 1
            x_copy(k).wait_recv()
            c_copy(k).start()

        @pl.when(jnp.logical_and(d >= 2, d < pieces + 2))
        def _():
            k = d - 2
            r1_copy(k).wait_recv()

            def add(j):
                total = part[k, other, j].astype(f32) + sum_in[k, 1 - hi, j].astype(f32)
                sum_send[k, j] = total.astype(bf16)

            across(add)
            r2_copy(k).start()

        at("home", lambda: near_home(1 - hi))
        at("home_own", lambda: near_home(hi))
        @pl.when(jnp.logical_and(d >= 3, d < pieces + 3))
        def _():
            k = d - 3
            r2_copy(k).wait_recv()

            def add(j):
                total = part[k, mine, j].astype(f32) + sum_in[k, hi, j].astype(f32) + cross_in[k, j].astype(f32)
                done_out[k, j] = total.astype(bf16)

            across(add)
            across(lambda j: r3_copy(k, j).start())

        if pieces > 2:
            @pl.when(d == 1)
            def _():
                arrive(2)

        def share():
            near_far().wait_recv()
            near_share(1 - hi).start()
            for stage in stages:
                near_own(*stage).wait_recv()
            near_share(hi).start()

        at("share", share)

        @pl.when(d < pieces + 1)
        def _():
            k = d - 1
            b_copy(k).wait_recv()
            c_copy(k).wait_recv()
            experts_of(k)
            r1_copy(k).start()

        @pl.when(jnp.logical_and(d >= 2, d < pieces - 1))
        def _():
            arrive(d + 1)

        def total_local():
            for h in range(2):
                def put(c, y):
                    near_back[h, c, 0] = y

                near_total(0, h, put)

        at("expert", lambda: near_expert(1 - hi))
        at("local", local_expert)
        at("total", total_local)
        at("expert_own", lambda: near_expert(hi))
        at("cross", lambda: far_combine(0))
        at("cross2", lambda: far_combine(1))
        return 0

    lax.fori_loop(1, turns, turn, 0)
    for k in range(max(pieces - 1, 0)):
        give_back(k)
    for c in range(2):
        def put(n, y):
            q = slice(c * half + n, c * half + n + wide)
            own[:, q] = own[:, q] + y

        near_combine(hi, c, put)
    for k in range(max(pieces - 1, 0), pieces):
        give_back(k)
    for c in range(2):
        dense_copy(c).wait_recv()

    finals = []
    for j in range(CHUNKS):
        q = slice(j * step, (j + 1) * step)
        crossed = jnp.concatenate([dense_in[0, q, :], dense_in[1, q, :]], axis=1).astype(f32)
        out[q, :] = layer_norm(own[q, :] + crossed, gain2[...], bias2[...]).astype(bf16)
        c = pltpu.make_async_copy(out.at[pl.ds(j * step, step)], out_h.at[pl.ds(j * step, step)], outs.at[j])
        c.start()
        finals.append(c)

    @pl.when(s < experts - 1)
    def _():
        for c in edges:
            c.wait_send()

    for c in beside + over + dense + swaps + [last, near_far()] + [near_own(*stage) for stage in stages]:
        c.wait_send()
    for h in range(2):
        for c in (local_copy(h), near_share(h), near_sum(0, h), near_sum(1, h), near_return(h, 0), near_return(h, 1), dense_copy(h)):
            c.wait_send()

    def drain(k):
        for c in (x_copy, b_copy, c_copy, r1_copy, r2_copy):
            c(k).wait_send()
        across(lambda i: z_out(k, i).wait_send())
        across(lambda j: r3_copy(k, j).wait_send())

    each(pieces, drain)
    for c in finals:
        c.wait()


def shards(
    gate_in, mult_in, value_in, doc_ids, conv_taps, out_proj, resid, norm1_gain, norm1_bias,
    expert_ids, expert_wts, w_gate, w_up, w_down, norm2_gain, norm2_bias,
):
    experts, parts = lax.axis_size("sp"), lax.axis_size("tp")
    assert parts == 4
    length, channels = mult_in.shape
    count, model = resid.shape
    top = expert_ids.shape[1]
    units = w_gate.shape[2]
    capacity = 5 * count * top // (4 * experts)
    piece = 16
    pieces = -(-capacity // piece)
    slots = pieces * piece
    padded = max(8, experts)
    others = experts - 2
    assert experts >= 4 and experts % 2 == 0
    hbm = pl.BlockSpec(memory_space=pl.ANY)
    V = pltpu.VMEM
    sems = pltpu.SemaphoreType.DMA
    blocks = (pieces, others, piece, model)
    routed = (pieces, 4, others, piece, model)
    batch = 4 * others * piece if 4 * others * piece <= 512 else others * piece
    batch = max(batch, 4 * slots)
    many, each_way = sems((pieces,)), sems((pieces, others))
    two, four = sems((2,)), sems((2, 2))
    return pl.pallas_call(
        functools.partial(kernel, experts, slots, piece),
        out_shape=jax.ShapeDtypeStruct((count, model), bf16),
        in_specs=[hbm] * 16,
        out_specs=hbm,
        scratch_shapes=[
            V((length, channels), bf16), V((length, channels), bf16), V((length, channels), bf16),
            V((1, length + 128), jnp.int32), V(conv_taps.shape, bf16), V((channels, model), bf16), V((count, model), bf16),
            V((1, model), f32), V((1, model), f32), V((top, count), jnp.int32), V((top, count), f32),
            V((model, units), bf16), V((model, units), bf16), V((units, model), bf16), V((1, model), f32), V((1, model), f32),
            V((16, channels), bf16), V((16, channels), bf16),
            V((length + 8, channels), f32), V((length + 8, 128), f32), V((length, channels), bf16),
            V((2, count, model), bf16), V((2, count, model), bf16), V((count, model), bf16), V((count, model), bf16),
            V((count, model), f32), V((count, model), bf16), V((count, model), bf16), V((count, model), bf16),
            V((top, count), jnp.int32), V((top, count), f32),
            V((2, padded, count), f32), V((2, padded, count), f32), V((2 * slots, count), bf16),
            V((pieces, experts, piece, count), bf16), V((2, 2 * slots, 2 * count), bf16), V((pieces, others, piece, 2 * count), bf16),
            V((2, 2, 2, slots, model), bf16), V((2, 2, 2, slots, model), bf16), V((2, slots, model), bf16),
            V((2, 2, slots, model), bf16), V((2, 2, slots, model // 2), bf16), V((2, 2, 2, slots, model // 2), bf16),
            V((2, count, model // 2), bf16), V((2, count, model // 2), bf16),
            V(blocks, bf16), V(routed, bf16), V(routed, bf16), V((batch, units), bf16),
            V((pieces, 2, others, piece, model), bf16), V(blocks, bf16), V(blocks, bf16), V(blocks, bf16),
            V(blocks, bf16),
            sems((16,)), sems((CHUNKS,)), sems((3,)), sems((3,)), sems((2 * CHUNKS + 1,)), sems((2 * CHUNKS + 1,)),
            two, two, sems((CHUNKS,)), sems((CHUNKS,)),
            two, two, sems((CHUNKS + 1,)), sems((CHUNKS + 1,)), two, two, four, four, four, four, two, two,
            each_way, each_way, many, many, many, many, many, many,
            many, many, many, many, each_way, each_way,
        ],
        compiler_params=pltpu.CompilerParams(
            collective_id=0, has_side_effects=True, vmem_limit_bytes=62 * 2**20
        ),
    )(
        gate_in, mult_in, value_in, doc_ids[None], conv_taps, out_proj, resid,
        norm1_gain[None], norm1_bias[None], expert_ids.T, expert_wts.T,
        w_gate[0], w_up[0], w_down[0], norm2_gain[None], norm2_bias[None],
    )


def solution(mesh):
    placed = (
        P(("grp", "sp"), "tp"),
        P(("grp", "sp"), "tp"),
        P(("grp", "sp"), "tp"),
        P(("grp", "sp")),
        P(None, "tp"),
        P("tp", None),
        P(("grp", "sp", "tp"), None),
        P(),
        P(),
        P(("grp", "sp", "tp"), None),
        P(("grp", "sp", "tp"), None),
        P("sp", None, "tp"),
        P("sp", None, "tp"),
        P("sp", "tp", None),
        P(),
        P(),
    )
    return jax.shard_map(
        shards, mesh=mesh, in_specs=placed, out_specs=P(("grp", "sp", "tp"), None), check_vma=False
    )
```

time: 98.3 us -> 87.4 us (0.89)
  Pallas kernels: 96.2 us -> 85.3 us
    pallas_call x1, Pallas kernels: 96.2 us -> 85.3 us  [shards(): pl.pallas_call(functools.partial(kernel, experts, slots, piece), out_shap...]
where the time goes in v2:
time: 87.4 us; the launch traced here: 87.2 us
  Pallas kernels  85.3 us (98%)
  local copies, waits for them, and re-layouts  1.88 us (2%)
    pallas_call x1, Pallas kernels, shards(): pl.pallas_call(functools.partial(kernel, experts, slots, piece), out_shap...  85.3 us
    unnamed x1, local copies, waits for them, and re-layouts  1.88 us

profile of v2, /device:TPU:0, one launch (start us, length us, event | category | flops | bytes accessed | tf_op | source)
XLA Modules:
  0.0 87.2 jit_solution(7005913093761182960)
XLA Ops:
  0.0 85.3 %shard_map.154 = bf16[128,2048]{1,0:T(8,128)(2,1)} custom-call(bf16[512,384]{1,0:T(8,128)(2,1)} %gate_h.1, bf16[512,384]{1,0:T(8,128)(2,1)} %mult_h.1, bf16[512,384]{1,0:T(8,128)(2,1)} %value_h.1, s32[1,512]{1,0:T(1,128)} %bitcast.17, bf16[3,384]{1,0:T(4,128)(2,1)} %taps_h.1, bf16[384,2048]{1,0:T(8,128)(2,1)} %proj_h.1, bf16[128,2048]{1,0:T(8,128)(2,1)} %resid_h.1, ...), custom_call_target="tpu_custom_call" | custom-call | tf_op jit(solution)/shard_map/pallas_call | solution.py:617
  85.3 1.9 %copy.18 = bf16[128,2048]{1,0:T(8,128)(2,1)} copy(bf16[128,2048]{1,0:T(8,128)(2,1)} %shard_map.154) | data formatting | bytes 1048576

commit v3 on v2

--- a/solution.py
+++ b/solution.py
@@ -298,7 +298,7 @@
         if ready[j] > begun:
             stages.append((j, begun, ready[j]))
             begun = ready[j]
-    held = max(pieces - 2, 1)
+    held = max(pieces - 1, 1)
 
     def near_share(h):
         block = rows_n.at[1, h, lo]
@@ -461,7 +461,9 @@
         near_sum(0, 0).start()
         near_sum(0, 1).start()
 
-    steps = {"share": 3, "expert": 3, "home": 4, "local": 4, "total": 5, "expert_own": 5, "home_own": 6, "cross": 6, "cross2": 6}
+    steps = {
+        "share_own": 1, "expert_own": 2, "home_own": 3, "share": 3, "expert": 3, "home": 4, "local": 4, "total": 5, "cross": 6, "cross2": 6
+    }
     turns = max(pieces + 3, max(steps.values()) + 1)
 
     def turn(d, _):
@@ -488,8 +490,8 @@
             across(add)
             r2_copy(k).start()
 
+        at("home_own", lambda: near_home(hi))
         at("home", lambda: near_home(1 - hi))
-        at("home_own", lambda: near_home(hi))
         @pl.when(jnp.logical_and(d >= 3, d < pieces + 3))
         def _():
             k = d - 3
@@ -507,9 +509,13 @@
             def _():
                 arrive(2)
 
+        at("expert_own", lambda: near_expert(hi))
+
         def share():
             near_far().wait_recv()
             near_share(1 - hi).start()
+
+        def share_own():
             for stage in stages:
                 near_own(*stage).wait_recv()
             near_share(hi).start()
@@ -528,6 +534,8 @@
         def _():
             arrive(d + 1)
 
+        at("share_own", share_own)
+
         def total_local():
             for h in range(2):
                 def put(c, y):
@@ -538,7 +546,6 @@
         at("expert", lambda: near_expert(1 - hi))
         at("local", local_expert)
         at("total", total_local)
-        at("expert_own", lambda: near_expert(hi))
         at("cross", lambda: far_combine(0))
         at("cross2", lambda: far_combine(1))
         return 0

time: 87.4 us -> 85.8 us (0.982)
  Pallas kernels: 85.3 us -> 83.7 us
    pallas_call x1, Pallas kernels: 85.3 us -> 83.7 us  [shards(): pl.pallas_call(functools.partial(kernel, experts, slots, piece), out_shap...]
where the time goes in v3:
time: 85.8 us; the launch traced here: 85.6 us
  Pallas kernels  83.7 us (98%)
  local copies, waits for them, and re-layouts  1.88 us (2%)
    pallas_call x1, Pallas kernels, shards(): pl.pallas_call(functools.partial(kernel, experts, slots, piece), out_shap...  83.7 us
    unnamed x1, local copies, waits for them, and re-layouts  1.88 us

profile of v3, /device:TPU:0, one launch (start us, length us, event | category | flops | bytes accessed | tf_op | source)
XLA Modules:
  0.0 85.6 jit_solution(7192399376938427343)
XLA Ops:
  0.0 83.7 %shard_map.154 = bf16[128,2048]{1,0:T(8,128)(2,1)} custom-call(bf16[512,384]{1,0:T(8,128)(2,1)} %gate_h.1, bf16[512,384]{1,0:T(8,128)(2,1)} %mult_h.1, bf16[512,384]{1,0:T(8,128)(2,1)} %value_h.1, s32[1,512]{1,0:T(1,128)} %bitcast.17, bf16[3,384]{1,0:T(4,128)(2,1)} %taps_h.1, bf16[384,2048]{1,0:T(8,128)(2,1)} %proj_h.1, bf16[128,2048]{1,0:T(8,128)(2,1)} %resid_h.1, ...), custom_call_target="tpu_custom_call" | custom-call | tf_op jit(solution)/shard_map/pallas_call | solution.py:624
  83.7 1.9 %copy.18 = bf16[128,2048]{1,0:T(8,128)(2,1)} copy(bf16[128,2048]{1,0:T(8,128)(2,1)} %shard_map.154) | data formatting | bytes 1048576

commit v4 on v3

--- a/solution.py
+++ b/solution.py
@@ -559,16 +559,16 @@
             own[:, q] = own[:, q] + y
 
         near_combine(hi, c, put)
-    for k in range(max(pieces - 1, 0), pieces):
-        give_back(k)
     for c in range(2):
         dense_copy(c).wait_recv()
+        q = slice(c * half, (c + 1) * half)
+        own[:, q] = own[:, q] + dense_in[c].astype(f32)
+    give_back(pieces - 1)
 
     finals = []
     for j in range(CHUNKS):
         q = slice(j * step, (j + 1) * step)
-        crossed = jnp.concatenate([dense_in[0, q, :], dense_in[1, q, :]], axis=1).astype(f32)
-        out[q, :] = layer_norm(own[q, :] + crossed, gain2[...], bias2[...]).astype(bf16)
+        out[q, :] = layer_norm(own[q, :], gain2[...], bias2[...]).astype(bf16)
         c = pltpu.make_async_copy(out.at[pl.ds(j * step, step)], out_h.at[pl.ds(j * step, step)], outs.at[j])
         c.start()
         finals.append(c)

time: 85.8 us -> 85.6 us (level)
  no operation moved by 1% of the time
where the time goes in v4:
time: 85.6 us; the launch traced here: 85.5 us
  Pallas kernels  83.6 us (98%)
  local copies, waits for them, and re-layouts  1.88 us (2%)
    pallas_call x1, Pallas kernels, shards(): pl.pallas_call(functools.partial(kernel, experts, slots, piece), out_shap...  83.6 us
    unnamed x1, local copies, waits for them, and re-layouts  1.88 us

profile of v4, /device:TPU:0, one launch (start us, length us, event | category | flops | bytes accessed | tf_op | source)
XLA Modules:
  0.0 85.5 jit_solution(7133947049203672956)
XLA Ops:
  0.0 83.6 %shard_map.154 = bf16[128,2048]{1,0:T(8,128)(2,1)} custom-call(bf16[512,384]{1,0:T(8,128)(2,1)} %gate_h.1, bf16[512,384]{1,0:T(8,128)(2,1)} %mult_h.1, bf16[512,384]{1,0:T(8,128)(2,1)} %value_h.1, s32[1,512]{1,0:T(1,128)} %bitcast.17, bf16[3,384]{1,0:T(4,128)(2,1)} %taps_h.1, bf16[384,2048]{1,0:T(8,128)(2,1)} %proj_h.1, bf16[128,2048]{1,0:T(8,128)(2,1)} %resid_h.1, ...), custom_call_target="tpu_custom_call" | custom-call | tf_op jit(solution)/shard_map/pallas_call | solution.py:624
  83.6 1.9 %copy.18 = bf16[128,2048]{1,0:T(8,128)(2,1)} copy(bf16[128,2048]{1,0:T(8,128)(2,1)} %shard_map.154) | data formatting | bytes 1048576
